TPU v7x, 128 devices: a whole 4x4x4 slice. The times are simulated.
128 devices in a mesh: sp: 16 (over z, x), fs: 4 (over y), tp: 2 (over core).
Axes of the slice: x: 4, y: 4, z: 4, core: 2. Of those that a mesh axis runs over, the one named last changes fastest.
Arguments:
- tokens: bfloat16 [4, 8192, 2048], P('fs', 'sp', 'tp'), may hold values from -6 to 6
- norm_gain: float32 [2048], replicated, may hold values from 0.1 to 1.9
- w_pool_in: bfloat16 [2048, 512], P('fs', 'tp'), may hold values from -0.125 to 0.125
- w_query: bfloat16 [2048, 1024], P('fs', 'tp'), may hold values from -0.125 to 0.125
- w_key: bfloat16 [2048, 1024], P('fs', 'tp'), may hold values from -0.125 to 0.125
- w_value: bfloat16 [2048, 1024], P('fs', 'tp'), may hold values from -0.125 to 0.125
- query_gain: float32 [64], replicated, may hold values from 1.5 to 2.5
- key_gain: float32 [64], replicated, may hold values from 1.5 to 2.5
- stick_offset: float32 [16], P('tp'), as said below
- pool_mix: bfloat16 [4, 128, 128], P('tp'), may hold values from -0.5 to 0.5
- pool_scale: float32 [512], P('tp'), may hold values from 0.2 to 4, as said below
- pool_gain: bfloat16 [512], P('tp'), may hold values from 0.099609375 to 1.8984375
- attn_gain: bfloat16 [1024], P('tp'), may hold values from 0.099609375 to 1.8984375
- w_out_pool: bfloat16 [512, 2048], P('tp', 'fs'), may hold values from -0.15625 to 0.15625
- w_out_attn: bfloat16 [1024, 2048], P('tp', 'fs'), may hold values from -0.15625 to 0.15625
Outputs:
- mixed: bfloat16 [4, 8192, 2048], P('fs', ('sp', 'tp'))
Inputs may be any that keep to these rules, and one draw needn't show every extreme that they name: `stick_offset`: per head, negative. `pool_scale`: positive channel scales.
All inputs are finite; a program needn't handle non-finite values.
Results may differ from a plain program's by a relative error of at most 0.013.
Values may be sent and summed in bfloat16 or wider, within the bound.
A program may use at most 192 MiB of HBM per device.

v0:
```python
import math
import jax
import jax.numpy as jnp
from jax import lax
from jax.sharding import PartitionSpec as P

HEADS = 16
HEAD_DIM = 64
POOL = 512
POOL_GROUPS = 4
EPS = 1e-06


def sent_to_all(shard, axis):
    devices = lax.axis_size(axis)
    return lax.all_to_all(
        jnp.broadcast_to(shard[None], (devices, *shard.shape)), axis, 0, 0, tiled=True
    )


def in_order(parts, dim):
    lengths = list(parts.shape[1:])
    lengths[dim] *= parts.shape[0]
    return jnp.moveaxis(parts, 0, dim).reshape(lengths)


def gathered_copies(shard, axis, dim):
    parts = sent_to_all(shard, axis)
    return in_order(parts, dim)


def in_one_piece(arrays, axis, dim, along):
    both = jnp.concatenate(arrays, axis=along)
    whole, at, outs = (lax.all_gather(both, axis, axis=dim, tiled=True), 0, [])
    for a in arrays:
        outs.append(lax.slice_in_dim(whole, at, at + a.shape[along], axis=along))
        at += a.shape[along]
    return tuple(outs)


def shifted_2(value, axis, steps):
    count = lax.axis_size(axis)
    initial, last = (max(0, -steps), min(count, count - steps))
    return lax.ppermute(value, axis, [(source, source + steps) for source in range(initial, last)])


def partner_2(shard, axis, distance):
    return lax.ppermute(shard, axis, [(i, i ^ 1 << distance) for i in range(lax.axis_size(axis))])


def head_norm(projected, gain, head_count):
    split = projected.reshape(projected.shape[0], head_count, HEAD_DIM)
    factor = lax.rsqrt(jnp.mean(split * split, axis=-1, keepdims=True) + EPS)
    return (split * factor * gain).astype(jnp.bfloat16)


def stick_block(query, key_heads, value_heads, offset, carried, row_offset, score_scale):
    scores = (
        jnp.einsum("thd,khd->htk", query, key_heads, preferred_element_type=jnp.float32)
        * score_scale
        + offset[:, None, None]
    )
    keep = jax.nn.log_sigmoid(-scores)
    if row_offset is not None:
        shape = (query.shape[0], key_heads.shape[0])
        earlier = (
            lax.broadcasted_iota(jnp.int32, shape, 1)
            < lax.broadcasted_iota(jnp.int32, shape, 0) + row_offset
        )
        keep = jnp.where(earlier[None], keep, 0.0)
    running = jnp.cumsum(keep, axis=2)
    block_total = running[:, :, -1]
    log_weight = (
        jax.nn.log_sigmoid(scores) + block_total[:, :, None] - running + carried[:, :, None]
    )
    weight = jnp.exp(log_weight)
    if row_offset is not None:
        weight = jnp.where(earlier[None], weight, 0.0)
    weight = weight.astype(jnp.bfloat16)
    block_out = jnp.einsum("htk,khd->thd", weight, value_heads, preferred_element_type=jnp.float32)
    return (block_out, block_total)


def branch_norm(values_in, squares, width, gain):
    values_f = values_in.astype(jnp.float32)
    factor = lax.rsqrt(squares / width + EPS)
    return (values_f * factor[:, None] * gain.astype(jnp.float32)).astype(jnp.bfloat16)


def shards(
    tokens,
    norm_gain,
    w_pool_in,
    w_query,
    w_key,
    w_value,
    query_gain,
    key_gain,
    stick_offset,
    pool_mix,
    pool_scale,
    pool_gain,
    attn_gain,
    w_out_pool,
    w_out_attn,
):
    whole = gathered_copies(tokens, "tp", 2)[0]
    whole_f = whole.astype(jnp.float32)
    normed = (
        whole_f * lax.rsqrt(jnp.mean(whole_f * whole_f, axis=-1, keepdims=True) + EPS) * norm_gain
    ).astype(jnp.bfloat16)
    row_count = normed.shape[0]
    pieces = in_one_piece((w_pool_in, w_query, w_key, w_value), "fs", 0, 1)
    pool_raw, query_raw, key_raw, value_raw = tuple(
        (jnp.dot(normed, piece, preferred_element_type=jnp.float32) for piece in pieces)
    )
    head_count = query_raw.shape[1] // HEAD_DIM
    query = head_norm(query_raw, query_gain, head_count)
    key_heads = head_norm(key_raw, key_gain, head_count)
    value_heads = value_raw.astype(jnp.bfloat16).reshape(row_count, head_count, HEAD_DIM)
    reach = 16
    pool_in = pool_raw.astype(jnp.bfloat16)
    previous = shifted_2(pool_in[row_count - reach :], "sp", 1)
    extended = jnp.concatenate([previous, pool_in], axis=0).astype(jnp.float32)
    pool_cols = pool_in.shape[1]
    group_ch = POOL // POOL_GROUPS
    local_groups = pool_cols // group_ch
    group_ids = (
        lax.axis_index("tp") * local_groups + jnp.arange(pool_cols, dtype=jnp.int32) // group_ch
    )
    window = jnp.left_shift(jnp.int32(2), group_ids)
    summed = jnp.zeros((row_count, pool_cols), jnp.float32)
    for behind in range(reach):
        shifted = extended[reach - behind : reach - behind + row_count]
        summed = summed + jnp.where(behind < window[None, :], shifted, 0.0)
    sp_index = lax.axis_index("sp")
    position = sp_index * row_count + jnp.arange(row_count, dtype=jnp.int32)
    counted = jnp.minimum(position[:, None] + 1, window[None, :]).astype(jnp.float32)
    centered = (summed / counted - extended[reach:]).astype(jnp.bfloat16)
    pooled = jnp.einsum(
        "tgc,gcd->tgd",
        centered.reshape(row_count, local_groups, group_ch),
        pool_mix,
        preferred_element_type=jnp.float32,
    )
    pool_out = (pooled.reshape(row_count, pool_cols) * pool_scale).astype(jnp.bfloat16)
    score_scale = 1.0 / math.sqrt(HEAD_DIM)
    sp_count = lax.axis_size("sp")
    key_value = jnp.stack([key_heads, value_heads])
    everything = lax.all_gather(key_value, "sp", axis=1, tiled=True)
    half = row_count // 2
    bit_count = sp_count.bit_length() - 1

    def run_rows(query_rows, source, row_offset):
        start_carry = jnp.zeros((head_count, query_rows.shape[0]), jnp.float32)
        diagonal = lax.dynamic_slice_in_dim(everything, source * row_count, row_count, 1)
        first_out, first_carry = stick_block(
            query_rows, diagonal[0], diagonal[1], stick_offset, start_carry, row_offset, score_scale
        )

        def turn(turn_index, state):
            acc_out, acc_carry = state
            block = lax.dynamic_slice_in_dim(
                everything, (source - turn_index) * row_count, row_count, 1
            )
            block_out, block_total = stick_block(
                query_rows, block[0], block[1], stick_offset, acc_carry, None, score_scale
            )
            return (acc_out + block_out, acc_carry + block_total)

        result, unused = lax.fori_loop(1, source + 1, turn, (first_out, first_carry))
        return result.reshape(query_rows.shape[0], head_count * HEAD_DIM).astype(jnp.bfloat16)

    guest_query = query[half:]
    for bit in range(bit_count):
        guest_query = partner_2(guest_query, "sp", bit)
    partner = sp_count - 1 - sp_index
    own_rows = run_rows(query[:half], sp_index, 0)
    guest_rows = run_rows(guest_query, partner, half)
    for bit in range(bit_count):
        guest_rows = partner_2(guest_rows, "sp", bit)
    attn_out = jnp.concatenate([own_rows, guest_rows], axis=0)
    w_pool_cols, w_attn_cols = (
        lax.all_gather(w_out_pool, "fs", axis=1, tiled=True),
        lax.all_gather(w_out_attn, "fs", axis=1, tiled=True),
    )
    pool_rows, attn_rows = (
        lax.all_to_all(pool_out, "tp", split_axis=0, concat_axis=1, tiled=True),
        lax.all_to_all(attn_out, "tp", split_axis=0, concat_axis=1, tiled=True),
    )
    w_pool_all, w_attn_all, pool_gain_all, attn_gain_all = (
        lax.all_gather(w_pool_cols, "tp", axis=0, tiled=True),
        lax.all_gather(w_attn_cols, "tp", axis=0, tiled=True),
        lax.all_gather(pool_gain, "tp", axis=0, tiled=True),
        lax.all_gather(attn_gain, "tp", axis=0, tiled=True),
    )
    pool_f = pool_rows.astype(jnp.float32)
    attn_f = attn_rows.astype(jnp.float32)
    pool_normed = branch_norm(pool_rows, jnp.sum(pool_f * pool_f, axis=-1), POOL, pool_gain_all)
    attn_normed = branch_norm(
        attn_rows, jnp.sum(attn_f * attn_f, axis=-1), HEADS * HEAD_DIM, attn_gain_all
    )
    mixed = jnp.dot(pool_normed, w_pool_all, preferred_element_type=jnp.float32) + jnp.dot(
        attn_normed, w_attn_all, preferred_element_type=jnp.float32
    )
    return mixed.astype(jnp.bfloat16)[None]


def solution(mesh):
    in_specs = (
        P("fs", "sp", "tp"),
        P(),
        P("fs", "tp"),
        P("fs", "tp"),
        P("fs", "tp"),
        P("fs", "tp"),
        P(),
        P(),
        P("tp"),
        P("tp", None, None),
        P("tp"),
        P("tp"),
        P("tp"),
        P("tp", "fs"),
        P("tp", "fs"),
    )
    out_specs = P("fs", ("sp", "tp"), None)
    return jax.shard_map(shards, mesh=mesh, in_specs=in_specs, out_specs=out_specs, check_vma=False)
```

profile of v0, /device:TPU:103, one launch (start us, length us, event | category | flops | bytes accessed | tf_op | source)
XLA Modules:
  0.0 761.2 jit_solution(1497514801564157925)
XLA Ops:
  6.5 2.9 pad_maximum_fusion
  11.9 5.5 all-to-all-start
  20.0 3.0 copy.102
  27.3 57.7 %all-gather.9.cloned.1.call-done = bf16[2048,1792]{1,0:T(8,128)(2,1)} async-done(((bf16[512,1792]{1,0:T(8,128)(2,1)}), bf16[2048,1792]{1,0:T(8,128)(2,1)}) %all-gather.9.cloned.1.call-update) | async-done | bytes 7340048 | tf_op jit(solution)/shard_map/all_gather | solution.py:34
  85.0 3.9 slice_bitcast_fusion.5
  88.9 4.0 copy.106
  92.9 3.6 multiply_reduce_fusion.2
  96.8 3.0 fusion.82
  101.0 17.3 %all-gather.17.cloned.1.call-done = bf16[512,2048]{1,0:T(8,128)(2,1)} async-done(((bf16[512,512]{1,0:T(8,128)(2,1)}), bf16[512,2048]{1,0:T(8,128)(2,1)}) %all-gather.17.cloned.1.call-update) | async-done | bytes 2097168 | tf_op jit(solution)/shard_map/all_gather | solution.py:185
  121.2 3.6 multiply_reduce_fusion.1
  134.2 8.0 %all-gather.11.cloned.1.call-done = bf16[256,2048]{1,0:T(8,128)(2,1)} async-done(((bf16[256,512]{1,0:T(8,128)(2,1)}), bf16[256,2048]{1,0:T(8,128)(2,1)}) %all-gather.11.cloned.1.call-update) | async-done | bytes 1048592 | tf_op jit(solution)/shard_map/all_gather | solution.py:184
  146.6 6.6 all-to-all-start.1
  154.5 8.8 %collective-permute-done.3 = bf16[256,8,64]{0,2,1:T(8,128)(2,1)S(1)} collective-permute-done((bf16[256,8,64]{0,2,1:T(8,128)(2,1)S(1)}, bf16[256,8,64]{0,2,1:T(8,128)(2,1)S(1)}, u32[]{:S(2)}, u32[]{:S(2)}) %collective-permute-start.3) | collective-permute-done | bytes 262176 | tf_op jit(solution)/shard_map/ppermute | solution.py:48
  165.4 5.4 collective-permute-done.4
  170.8 97.9 %all-gather.15.cloned.1.call-done = bf16[2,8192,8,64]{1,3,2,0:T(8,128)(2,1)} async-done(((bf16[2,512,8,64]{1,3,2,0:T(8,128)(2,1)}), bf16[2,8192,8,64]{1,3,2,0:T(8,128)(2,1)}) %all-gather.15.cloned.1.call-update) | async-done | bytes 16777232 | tf_op jit(solution)/shard_map/all_gather | solution.py:150
  270.6 10.6 %fusion.63 = (f32[8,256,512]{2,1,0:T(8,128)}, f32[8,256,512]{2,1,0:T(8,128)}, f32[8,256,512]{2,1,0:T(8,128)}) fusion(f32[8]{0:T(128)S(1)} %copy-done.14, pred[256,512]{1,0:T(8,128)(4,1)S(1)} %get-tuple-element.157, f32[8,256,512]{2,1,0:T(8,128)S(1)} %fusion.97, pred[256,512]{1,0:T(8,128)(4,1)S(1)} %get-tuple-element.156, ...), kind=kOutput, calls=%fused_computation.79 | convolution fusion | flops 155189248 | bytes 17826308 | tf_op jit(solution)/shard_map/thd,khd->htk/dot_general | solution.py:59
  281.2 5.7 copy.122
  286.9 5.6 copy.124
  297.5 5.3 copy.125
  304.8 6.4 fusion.88
  311.4 14.4 %collective-permute-start.5 = (bf16[256,512]{0,1:T(8,128)(2,1)S(1)}, bf16[256,512]{0,1:T(8,128)(2,1)S(1)}, u32[]{:S(2)}, u32[]{:S(2)}) collective-permute-start(bf16[256,512]{0,1:T(8,128)(2,1)S(1)} %bitcast.254), channel_id=1, source_target_pairs={{0,8},{8,0},{16,24},{24,16},{32,40},{40,32},{48,56},{56,48},{64,72... | collective-permute-start | bytes 786440 | tf_op jit(solution)/shard_map/ppermute | solution.py:48
  330.5 28.5 %collective-permute-start.6 = (bf16[256,512]{0,1:T(8,128)(2,1)S(1)}, bf16[256,512]{0,1:T(8,128)(2,1)S(1)}, u32[]{:S(2)}, u32[]{:S(2)}) collective-permute-start(bf16[256,512]{0,1:T(8,128)(2,1)S(1)} %collective-permute-done.5), channel_id=1, source_target_pairs={{0,16},{8,24},{16,0},{24,8},{32,48},{40,56},{48,32},{56,40},{64,80... | collective-permute-start | bytes 786440 | tf_op jit(solution)/shard_map/ppermute | solution.py:48
  361.2 5.3 copy.123
  368.3 53.3 %collective-permute-start.7 = (bf16[256,512]{0,1:T(8,128)(2,1)S(1)}, bf16[256,512]{0,1:T(8,128)(2,1)S(1)}, u32[]{:S(2)}, u32[]{:S(2)}) collective-permute-start(bf16[256,512]{0,1:T(8,128)(2,1)S(1)} %collective-permute-done.6), channel_id=1, source_target_pairs={{0,32},{8,40},{16,48},{24,56},{32,0},{40,8},{48,16},{56,24},{64,96... | collective-permute-start | bytes 786440 | tf_op jit(solution)/shard_map/ppermute | solution.py:48
  421.7 6.4 fusion.85
  428.1 110.3 %collective-permute-start.8 = (bf16[256,512]{0,1:T(8,128)(2,1)S(1)}, bf16[256,512]{0,1:T(8,128)(2,1)S(1)}, u32[]{:S(2)}, u32[]{:S(2)}) collective-permute-start(bf16[256,512]{0,1:T(8,128)(2,1)S(1)} %collective-permute-done.7), channel_id=1, source_target_pairs={{0,64},{8,72},{16,80},{24,88},{32,96},{40,104},{48,112},{56,120},{... | collective-permute-start | bytes 786440 | tf_op jit(solution)/shard_map/ppermute | solution.py:48
  538.4 200.5 %while.24 = (s32[]{:T(128)}, f32[256,8,64]{0,2,1:T(8,128)S(1)}, f32[8,256]{1,0:T(8,128)S(1)}, s32[]{:T(128)}, s32[]{:T(128)}, /*index=5*/bf16[2,8192,8,64]{1,3,2...) while((s32[]{:T(128)}, f32[256,8,64]{0,2,1:T(8,128)S(1)}, ...), condition=%wide.region_9.10_spmd, body=%wide.region_6.9_spmd.sunk | while | flops 426934272 | bytes 44548372 | solution.py:171
  538.4 4.1 fusion.176
  542.5 2.6 fusion.177
  547.0 4.7 fusion.179
  551.8 4.1 fusion.176
  555.9 2.6 fusion.177
  560.4 4.7 fusion.179
  565.2 4.1 fusion.176
  573.7 4.7 fusion.179
  578.5 4.1 fusion.176
  587.1 4.7 fusion.179
  591.9 4.1 fusion.176
  596.0 2.6 fusion.177
  600.5 4.7 fusion.179
  605.3 4.1 fusion.176
  613.8 4.7 fusion.179
  618.6 4.1 fusion.176
  627.2 4.7 fusion.179
  632.0 4.1 fusion.176
  640.6 4.7 fusion.179
  645.4 4.1 fusion.176
  653.9 4.7 fusion.179
  658.7 4.1 fusion.176
  667.3 4.7 fusion.179
  672.1 4.1 fusion.176
  680.7 4.7 fusion.179
  685.5 4.1 fusion.176
  694.1 4.7 fusion.179
  698.8 4.1 fusion.176
  707.4 4.7 fusion.179
  712.2 4.1 fusion.176
  716.3 2.6 fusion.177
  720.8 4.7 fusion.179
  725.6 4.1 fusion.176
  734.2 4.7 fusion.179
  739.3 6.9 all_to_all.28
  747.1 3.5 fusion.138
  750.6 3.3 fusion.75
  (238 shorter events, 105.8 us)
Async XLA Ops:
  6.5 137.0 %copy-start = (bf16[2,128,128]{2,1,0:T(8,128)(2,1)S(1)}, bf16[2,128,128]{2,1,0:T(8,128)(2,1)}, u32[]{:S(2)}) copy-start(bf16[2,128,128]{2,1,0:T(8,128)(2,1)} %param.28) | copy-start | bytes 196612
  6.5 3.7 copy-start.5
  6.5 78.5 %all-gather.9.cloned.1.call-start = ((), (), s32[]{:S(2)}) async-start(), calls=%async_computation.3 | async-start | bytes 9175040 | tf_op jit(solution)/shard_map/all_gather | solution.py:34
  9.5 8.7 %copy-start.7 = (f32[2048]{0:T(1024)S(1)}, f32[2048]{0:T(1024)}, u32[]{:S(2)}) copy-start(f32[2048]{0:T(1024)} %param.20) | copy-start | bytes 24580
  9.5 108.8 %all-gather.17.cloned.1.call-start = ((), (), s32[]{:S(2)}) async-start(), calls=%async_computation.7 | async-start | bytes 2621440 | tf_op jit(solution)/shard_map/all_gather | solution.py:185
  11.9 8.1 %all-to-all-start = ((bf16[2,1,512,1024]{3,2,1,0:T(8,128)(2,1)}), bf16[2,1,512,1024]{3,2,1,0:T(8,128)(2,1)}, u32[]{:S(2)}, u32[]{:S(2)}) async-start(bf16[2,1,512,1024]{3,2,1,0:T(8,128)(2,1)} %broadcast_in_dim.182), calls=%async_computation | async-start | bytes 4194304 | tf_op jit(solution)/shard_map/all_to_all | solution.py:16
  17.4 124.8 %all-gather.11.cloned.1.call-start = ((), (), s32[]{:S(2)}) async-start(), calls=%async_computation.4 | async-start | bytes 1310720 | tf_op jit(solution)/shard_map/all_gather | solution.py:184
  18.1 250.7 %all-gather.15.cloned.1.call-start = ((), (), s32[]{:S(2)}) async-start(), calls=%async_computation.6 | async-start | bytes 17825792 | tf_op jit(solution)/shard_map/all_gather | solution.py:150
  92.9 3.7 copy-start.11
  92.9 3.9 copy-start.3
  100.9 646.2 %all-gather.19.cloned.1.call-start = ((), (), s32[]{:S(2)}) async-start(), calls=%async_computation.8 | async-start | bytes 6291456 | tf_op jit(solution)/shard_map/all_gather | solution.py:193
  118.3 632.3 %all-gather.13.cloned.1.call-start = ((), (), s32[]{:S(2)}) async-start(), calls=%async_computation.5 | async-start | bytes 3145728 | tf_op jit(solution)/shard_map/all_gather | solution.py:192
  121.2 3.7 copy-start.12
  121.2 4.6 copy-start.4
  124.9 4.3 copy-start.13
  124.9 6.9 copy-start.10
  125.2 17.1 %collective-permute-start.1 = (bf16[256,8,64]{0,2,1:T(8,128)(2,1)S(1)}, bf16[256,8,64]{0,2,1:T(8,128)(2,1)S(1)}, u32[]{:S(2)}, u32[]{:S(2)}) collective-permute-start(bf16[256,8,64]{0,2,1:T(8,128)(2,1)S(1)} %get-tuple-element.132), channel_id=1, source_target_pairs={{0,8},{8,0},{16,24},{24,16},{32,40},{40,32},{48,56},{56,48},{64,72... | collective-permute-start | bytes 786440 | tf_op jit(solution)/shard_map/ppermute | solution.py:48
  127.9 14.4 %collective-permute-start = (bf16[16,256]{1,0:T(8,128)(2,1)S(1)}, bf16[16,256]{1,0:T(8,128)(2,1)S(1)}, u32[]{:S(2)}, u32[]{:S(2)}) collective-permute-start(bf16[16,256]{1,0:T(8,128)(2,1)S(1)} %slice.170), channel_id=1, source_target_pairs={{0,8},{8,16},{16,24},{24,32},{32,40},{40,48},{48,56},{56,64},{64,7... | collective-permute-start | bytes 24584 | tf_op jit(solution)/shard_map/ppermute | solution.py:44
  142.3 10.9 %collective-permute-start.2 = (bf16[256,8,64]{0,2,1:T(8,128)(2,1)S(1)}, bf16[256,8,64]{0,2,1:T(8,128)(2,1)S(1)}, u32[]{:S(2)}, u32[]{:S(2)}) collective-permute-start(bf16[256,8,64]{0,2,1:T(8,128)(2,1)S(1)} %collective-permute-done.1), channel_id=1, source_target_pairs={{0,16},{8,24},{16,0},{24,8},{32,48},{40,56},{48,32},{56,40},{64,80... | collective-permute-start | bytes 786440 | tf_op jit(solution)/shard_map/ppermute | solution.py:48
  143.6 2.3 copy-start.9
  146.6 124.0 %copy-start.14 = (f32[8]{0:T(128)S(1)}, f32[8]{0:T(128)}, u32[]{:S(2)}) copy-start(f32[8]{0:T(128)} %param.27) | copy-start | bytes 100
  146.6 7.8 %all-to-all-start.1 = ((bf16[2,256,256]{2,1,0:T(8,128)(2,1)}), bf16[2,256,256]{2,1,0:T(8,128)(2,1)S(1)}, u32[]{:S(2)}, u32[]{:S(2)}) async-start(bf16[2,256,256]{2,1,0:T(8,128)(2,1)} %multiply_convert_fusion.3), calls=%async_computation.1 | async-start | bytes 524288 | tf_op jit(solution)/shard_map/all_to_all | solution.py:188
  153.2 10.2 %collective-permute-start.3 = (bf16[256,8,64]{0,2,1:T(8,128)(2,1)S(1)}, bf16[256,8,64]{0,2,1:T(8,128)(2,1)S(1)}, u32[]{:S(2)}, u32[]{:S(2)}) collective-permute-start(bf16[256,8,64]{0,2,1:T(8,128)(2,1)S(1)} %collective-permute-done.2), channel_id=1, source_target_pairs={{0,32},{8,40},{16,48},{24,56},{32,0},{40,8},{48,16},{56,24},{64,96... | collective-permute-start | bytes 786440 | tf_op jit(solution)/shard_map/ppermute | solution.py:48
  163.3 7.5 collective-permute-start.4
  270.6 10.6 %copy-start.2 = (f32[8,256,512]{2,1,0:T(8,128)}, f32[8,256,512]{2,1,0:T(8,128)S(1)}, u32[]{:S(2)}) copy-start(f32[8,256,512]{2,1,0:T(8,128)S(1)} %fusion.97) | copy-start | bytes 12582916
  311.4 19.1 %collective-permute-start.5 = (bf16[256,512]{0,1:T(8,128)(2,1)S(1)}, bf16[256,512]{0,1:T(8,128)(2,1)S(1)}, u32[]{:S(2)}, u32[]{:S(2)}) collective-permute-start(bf16[256,512]{0,1:T(8,128)(2,1)S(1)} %bitcast.254), channel_id=1, source_target_pairs={{0,8},{8,0},{16,24},{24,16},{32,40},{40,32},{48,56},{56,48},{64,72... | collective-permute-start | bytes 786440 | tf_op jit(solution)/shard_map/ppermute | solution.py:48
  330.5 37.8 %collective-permute-start.6 = (bf16[256,512]{0,1:T(8,128)(2,1)S(1)}, bf16[256,512]{0,1:T(8,128)(2,1)S(1)}, u32[]{:S(2)}, u32[]{:S(2)}) collective-permute-start(bf16[256,512]{0,1:T(8,128)(2,1)S(1)} %collective-permute-done.5), channel_id=1, source_target_pairs={{0,16},{8,24},{16,0},{24,8},{32,48},{40,56},{48,32},{56,40},{64,80... | collective-permute-start | bytes 786440 | tf_op jit(solution)/shard_map/ppermute | solution.py:48
  368.3 59.7 %collective-permute-start.7 = (bf16[256,512]{0,1:T(8,128)(2,1)S(1)}, bf16[256,512]{0,1:T(8,128)(2,1)S(1)}, u32[]{:S(2)}, u32[]{:S(2)}) collective-permute-start(bf16[256,512]{0,1:T(8,128)(2,1)S(1)} %collective-permute-done.6), channel_id=1, source_target_pairs={{0,32},{8,40},{16,48},{24,56},{32,0},{40,8},{48,16},{56,24},{64,96... | collective-permute-start | bytes 786440 | tf_op jit(solution)/shard_map/ppermute | solution.py:48
  428.1 310.9 %collective-permute-start.8 = (bf16[256,512]{0,1:T(8,128)(2,1)S(1)}, bf16[256,512]{0,1:T(8,128)(2,1)S(1)}, u32[]{:S(2)}, u32[]{:S(2)}) collective-permute-start(bf16[256,512]{0,1:T(8,128)(2,1)S(1)} %collective-permute-done.7), channel_id=1, source_target_pairs={{0,64},{8,72},{16,80},{24,88},{32,96},{40,104},{48,112},{56,120},{... | collective-permute-start | bytes 786440 | tf_op jit(solution)/shard_map/ppermute | solution.py:48
  738.9 7.9 %copy-start.8 = (f32[2,1,512]{2,1,0:T(1,128)S(1)}, f32[2,1,512]{2,1,0:T(1,128)}, u32[]{:S(2)}) copy-start(f32[2,1,512]{2,1,0:T(1,128)} %convert_element_type.154) | copy-start | bytes 12292
  746.9 3.8 copy-start.6
  747.1 6.8 copy-start.1
Sparse Core Ops, SparseCore 0:
  9.6 75.4 all-gather.8
  86.7 31.5 all-gather.16
  120.0 22.1 all-gather.10
  144.2 124.5 all-gather.14
  270.3 19.9 all-gather.18
  291.7 14.6 all-gather.12
where the time goes:
time: 772 us; the launch traced here: 761 us
  starting transfers between devices  224 us (29%)
  waiting for transfers between devices  201 us (26%)
  matrix products  178 us (23%)
  other arithmetic  68 us (9%)
  local copies, waits for them, and re-layouts  63.1 us (8%)
  between operations  14.4 us (2%)
  blocking collectives  11.4 us (1%)
    ppermute x8, starting transfers between devices, partner_2(): lax.ppermute(shard, axis, [(i, i ^ 1 << distance) for i in range(lax.axis...  210 us
    all_gather x1, waiting for transfers between devices, shards(): everything = lax.all_gather(key_value, 'sp', axis=1, tiled=True)  97.9 us
    dot_general x17, matrix products, stick_block(): jnp.einsum('htk,khd->thd', weight, value_heads, preferred_element_type=jn...  84 us
    dot_general x17, matrix products, stick_block(): jnp.einsum('thd,khd->htk', query, key_heads, preferred_element_type=jnp.f...  73.4 us
    another operation x52, other arithmetic  57.9 us
    all_gather x1, waiting for transfers between devices, in_one_piece(): whole, at, outs = (lax.all_gather(both, axis, axis=dim, tiled=True), 0, [])  57.7 us
    another operation x36, local copies, waits for them, and re-layouts  42.3 us
    all_gather x1, waiting for transfers between devices, shards(): lax.all_gather(w_out_attn, 'fs', axis=1, tiled=True)  17.3 us
  transfers between devices with their start and end apart: 17, of which 9 were waited for; matrix products, arithmetic and copies ran while one was open for 40% of the time, Pallas kernels for 0%

commit v1 on v0

--- a/solution.py
+++ b/solution.py
@@ -147,7 +147,12 @@
     score_scale = 1.0 / math.sqrt(HEAD_DIM)
     sp_count = lax.axis_size("sp")
     key_value = jnp.stack([key_heads, value_heads])
-    everything = lax.all_gather(key_value, "sp", axis=1, tiled=True)
+    ring = [key_value]
+    for hop in range(15):
+        ring.append(lax.ppermute(ring[-1], "sp", [(dev, (dev + 1) % 16) for dev in range(16)]))
+    everything = jnp.roll(
+        jnp.concatenate(ring[::-1], axis=1), (lax.axis_index("sp") + 1) * ring[0].shape[1], axis=1
+    )
     half = row_count // 2
     bit_count = sp_count.bit_length() - 1
 

time: 772 us -> 1020 us (1.32)
  waiting for transfers between devices: 201 us -> 292 us
  starting transfers between devices: 224 us -> 305 us
  local copies, waits for them, and re-layouts: 63.1 us -> 115 us
  blocking collectives: 11.4 us -> 31 us
    ppermute x0 -> x15, waiting for transfers between devices: none -> 218 us  [shards(): lax.ppermute(ring[-1], 'sp', [(dev, (dev + 1) % 16) for dev in range(16)])]
    all_gather x1 -> x0, waiting for transfers between devices: 97.9 us -> none  [shards(): everything = lax.all_gather(key_value, 'sp', axis=1, tiled=True)]
    ppermute x0 -> x15, starting transfers between devices: none -> 71.4 us  [shards(): lax.ppermute(ring[-1], 'sp', [(dev, (dev + 1) % 16) for dev in range(16)])]
    unnamed x32 -> x88, local copies, waits for them, and re-layouts: 0.08 us -> 38.7 us
    all_to_all x1, starting transfers between devices: 6.59 us -> 24.1 us  [shards(): lax.all_to_all(pool_out, 'tp', split_axis=0, concat_axis=1, tiled=True)]
    all_gather x1, waiting for transfers between devices: 17.3 us -> 0.01 us  [shards(): lax.all_gather(w_out_attn, 'fs', axis=1, tiled=True)]
    all_gather x1, blocking collectives: 2.59 us -> 15.5 us  [shards(): lax.all_gather(pool_gain, 'tp', axis=0, tiled=True)]
  transfers between devices with their start and end apart: 17 -> 31, of which waited for: 9 -> 19; matrix products, arithmetic and copies ran while one was open for 40% -> 34% of each run, Pallas kernels for 0% -> 0%
where the time goes in v1:
time: 1020 us; the launch traced here: 1010 us
  starting transfers between devices  305 us (30%)
  waiting for transfers between devices  292 us (29%)
  matrix products  181 us (18%)
  local copies, waits for them, and re-layouts  115 us (11%)
  other arithmetic  72.1 us (7%)
  blocking collectives  31 us (3%)
  between operations  14.3 us (1%)
    ppermute x15, waiting for transfers between devices, shards(): lax.ppermute(ring[-1], 'sp', [(dev, (dev + 1) % 16) for dev in range(16)])  218 us
    ppermute x8, starting transfers between devices, partner_2(): lax.ppermute(shard, axis, [(i, i ^ 1 << distance) for i in range(lax.axis...  203 us
    dot_general x17, matrix products, stick_block(): jnp.einsum('htk,khd->thd', weight, value_heads, preferred_element_type=jn...  84.5 us
    dot_general x17, matrix products, stick_block(): jnp.einsum('thd,khd->htk', query, key_heads, preferred_element_type=jnp.f...  75.7 us
    ppermute x15, starting transfers between devices, shards(): lax.ppermute(ring[-1], 'sp', [(dev, (dev + 1) % 16) for dev in range(16)])  71.4 us
    all_gather x1, waiting for transfers between devices, in_one_piece(): whole, at, outs = (lax.all_gather(both, axis, axis=dim, tiled=True), 0, [])  58.5 us
    another operation x52, other arithmetic  57.8 us
    another operation x36, local copies, waits for them, and re-layouts  41.8 us
  transfers between devices with their start and end apart: 31, of which 19 were waited for; matrix products, arithmetic and copies ran while one was open for 34% of the time, Pallas kernels for 0%

profile of v1, /device:TPU:103, one launch (start us, length us, event | category | flops | bytes accessed | tf_op | source)
XLA Modules:
  0.0 1013.1 jit_solution(9693493390536112752)
XLA Ops:
  11.1 5.5 all-to-all-start
  26.6 58.5 %all-gather.8.cloned.1.call-done = bf16[2048,1792]{1,0:T(8,128)(2,1)} async-done(((bf16[512,1792]{1,0:T(8,128)(2,1)}), bf16[2048,1792]{1,0:T(8,128)(2,1)}) %all-gather.8.cloned.1.call-update) | async-done | bytes 7340048 | tf_op jit(solution)/shard_map/all_gather | solution.py:34
  99.9 23.9 %collective-permute-done.1 = bf16[2,512,8,64]{1,3,2,0:T(8,128)(2,1)S(1)} collective-permute-done((bf16[2,512,8,64]{1,3,2,0:T(8,128)(2,1)S(1)}, bf16[2,512,8,64]{1,3,2,0:T(8,128)(2,1)S(1)}, u32[]{:S(2)}, u32[]{:S(2)}) %collective-permute-start.1) | collective-permute-done | bytes 1048608 | tf_op jit(solution)/shard_map/ppermute | solution.py:152
  128.1 20.8 %collective-permute-done.2 = bf16[2,512,8,64]{1,3,2,0:T(8,128)(2,1)S(1)} collective-permute-done((bf16[2,512,8,64]{1,3,2,0:T(8,128)(2,1)S(1)}, bf16[2,512,8,64]{1,3,2,0:T(8,128)(2,1)S(1)}, u32[]{:S(2)}, u32[]{:S(2)}) %collective-permute-start.2) | collective-permute-done | bytes 1048608 | tf_op jit(solution)/shard_map/ppermute | solution.py:152
  149.9 5.5 collective-permute-start.3
  155.4 20.0 %collective-permute-done.3 = bf16[2,512,8,64]{1,3,2,0:T(8,128)(2,1)} collective-permute-done((bf16[2,512,8,64]{1,3,2,0:T(8,128)(2,1)S(1)}, bf16[2,512,8,64]{1,3,2,0:T(8,128)(2,1)}, u32[]{:S(2)}, u32[]{:S(2)}) %collective-permute-start.3) | collective-permute-done | bytes 1048608 | tf_op jit(solution)/shard_map/ppermute | solution.py:152
  175.4 5.6 collective-permute-start.4
  181.1 19.4 %collective-permute-done.4 = bf16[2,512,8,64]{1,3,2,0:T(8,128)(2,1)} collective-permute-done((bf16[2,512,8,64]{1,3,2,0:T(8,128)(2,1)}, bf16[2,512,8,64]{1,3,2,0:T(8,128)(2,1)}, u32[]{:S(2)}, u32[]{:S(2)}) %collective-permute-start.4) | collective-permute-done | bytes 1048608 | tf_op jit(solution)/shard_map/ppermute | solution.py:152
  200.5 5.5 collective-permute-start.5
  206.0 18.6 %collective-permute-done.5 = bf16[2,512,8,64]{1,3,2,0:T(8,128)(2,1)S(1)} collective-permute-done((bf16[2,512,8,64]{1,3,2,0:T(8,128)(2,1)}, bf16[2,512,8,64]{1,3,2,0:T(8,128)(2,1)S(1)}, u32[]{:S(2)}, u32[]{:S(2)}) %collective-permute-start.5) | collective-permute-done | bytes 1048608 | tf_op jit(solution)/shard_map/ppermute | solution.py:152
  225.6 5.4 collective-permute-start.6
  231.0 17.4 %collective-permute-done.6 = bf16[2,512,8,64]{1,3,2,0:T(8,128)(2,1)} collective-permute-done((bf16[2,512,8,64]{1,3,2,0:T(8,128)(2,1)S(1)}, bf16[2,512,8,64]{1,3,2,0:T(8,128)(2,1)}, u32[]{:S(2)}, u32[]{:S(2)}) %collective-permute-start.6) | collective-permute-done | bytes 1048608 | tf_op jit(solution)/shard_map/ppermute | solution.py:152
  248.4 5.6 collective-permute-start.7
  254.1 16.8 %collective-permute-done.7 = bf16[2,512,8,64]{1,3,2,0:T(8,128)(2,1)} collective-permute-done((bf16[2,512,8,64]{1,3,2,0:T(8,128)(2,1)}, bf16[2,512,8,64]{1,3,2,0:T(8,128)(2,1)}, u32[]{:S(2)}, u32[]{:S(2)}) %collective-permute-start.7) | collective-permute-done | bytes 1048608 | tf_op jit(solution)/shard_map/ppermute | solution.py:152
  270.9 5.5 collective-permute-start.8
  276.4 16.1 %collective-permute-done.8 = bf16[2,512,8,64]{1,3,2,0:T(8,128)(2,1)} collective-permute-done((bf16[2,512,8,64]{1,3,2,0:T(8,128)(2,1)}, bf16[2,512,8,64]{1,3,2,0:T(8,128)(2,1)}, u32[]{:S(2)}, u32[]{:S(2)}) %collective-permute-start.8) | collective-permute-done | bytes 1048608 | tf_op jit(solution)/shard_map/ppermute | solution.py:152
  292.5 5.5 collective-permute-start.9
  298.1 16.0 %collective-permute-done.9 = bf16[2,512,8,64]{1,3,2,0:T(8,128)(2,1)} collective-permute-done((bf16[2,512,8,64]{1,3,2,0:T(8,128)(2,1)}, bf16[2,512,8,64]{1,3,2,0:T(8,128)(2,1)}, u32[]{:S(2)}, u32[]{:S(2)}) %collective-permute-start.9) | collective-permute-done | bytes 1048608 | tf_op jit(solution)/shard_map/ppermute | solution.py:152
  314.1 5.5 collective-permute-start.10
  319.6 16.1 %collective-permute-done.10 = bf16[2,512,8,64]{1,3,2,0:T(8,128)(2,1)} collective-permute-done((bf16[2,512,8,64]{1,3,2,0:T(8,128)(2,1)}, bf16[2,512,8,64]{1,3,2,0:T(8,128)(2,1)}, u32[]{:S(2)}, u32[]{:S(2)}) %collective-permute-start.10) | collective-permute-done | bytes 1048608 | tf_op jit(solution)/shard_map/ppermute | solution.py:152
  335.7 5.5 collective-permute-start.11
  341.2 16.1 %collective-permute-done.11 = bf16[2,512,8,64]{1,3,2,0:T(8,128)(2,1)} collective-permute-done((bf16[2,512,8,64]{1,3,2,0:T(8,128)(2,1)}, bf16[2,512,8,64]{1,3,2,0:T(8,128)(2,1)}, u32[]{:S(2)}, u32[]{:S(2)}) %collective-permute-start.11) | collective-permute-done | bytes 1048608 | tf_op jit(solution)/shard_map/ppermute | solution.py:152
  357.3 5.5 collective-permute-start.12
  362.9 15.5 %all-gather = bf16[2,1,256]{2,1,0:T(2,128)(2,1)S(1)} all-gather(bf16[1,1,256]{2,1,0:T(2,128)(2,1)S(1)} %reshape.262), channel_id=1, replica_groups=mesh['sp'=16,'fs'=4,'tp'=2] {'tp'}, dimensions={0}, use_global_device_ids=true | all-gather | bytes 1536 | tf_op jit(solution)/shard_map/all_gather | solution.py:199
  395.2 5.7 collective-permute-done.13
  400.9 5.2 collective-permute-start.14
  412.2 11.5 %collective-permute-done.14 = bf16[2,512,8,64]{1,3,2,0:T(8,128)(2,1)S(1)} collective-permute-done((bf16[2,512,8,64]{1,3,2,0:T(8,128)(2,1)}, bf16[2,512,8,64]{1,3,2,0:T(8,128)(2,1)S(1)}, u32[]{:S(2)}, u32[]{:S(2)}) %collective-permute-start.14) | collective-permute-done | bytes 1048608 | tf_op jit(solution)/shard_map/ppermute | solution.py:152
  423.7 5.1 collective-permute-start.15
  430.6 24.1 %all-to-all-start.1 = ((bf16[2,256,256]{2,1,0:T(8,128)(2,1)}), bf16[2,256,256]{2,1,0:T(8,128)(2,1)S(1)}, u32[]{:S(2)}, u32[]{:S(2)}) async-start(bf16[2,256,256]{2,1,0:T(8,128)(2,1)} %multiply_convert_fusion.3), calls=%async_computation.1 | async-start | bytes 524288 | tf_op jit(solution)/shard_map/all_to_all | solution.py:193
  456.8 7.4 collective-permute-done.17
  503.4 8.9 constant_dynamic-slice_fusion
  516.2 4.7 copy-done.2
  520.9 10.8 %fusion.63 = (f32[8,256,512]{2,1,0:T(8,128)}, f32[8,256,512]{2,1,0:T(8,128)}, f32[8,256,512]{2,1,0:T(8,128)}) fusion(f32[8]{0:T(128)S(1)} %copy-done.24, pred[256,512]{1,0:T(8,128)(4,1)S(1)} %copy-done.15, f32[8,256,512]{2,1,0:T(8,128)} %fusion.97, pred[256,512]{1,0:T(8,128)(4,1)S(1)} %copy-done.16, ...), kind=kOutput, calls=%fused_computation.79 | convolution fusion | flops 155189248 | bytes 17826308 | tf_op jit(solution)/shard_map/thd,khd->htk/dot_general | solution.py:59
  531.7 5.5 copy.122
  537.1 5.5 copy.124
  547.5 5.3 copy.125
  554.7 6.7 fusion.88
  561.6 9.7 collective-permute-start.20
  575.0 30.0 %collective-permute-start.21 = (bf16[256,512]{0,1:T(8,128)(2,1)S(1)}, bf16[256,512]{0,1:T(8,128)(2,1)S(1)}, u32[]{:S(2)}, u32[]{:S(2)}) collective-permute-start(bf16[256,512]{0,1:T(8,128)(2,1)S(1)} %collective-permute-done.20), channel_id=1, source_target_pairs={{0,16},{8,24},{16,0},{24,8},{32,48},{40,56},{48,32},{56,40},{64,80... | collective-permute-start | bytes 786440 | tf_op jit(solution)/shard_map/ppermute | solution.py:48
  607.4 5.2 copy.123
  614.5 55.0 %collective-permute-start.22 = (bf16[256,512]{0,1:T(8,128)(2,1)S(1)}, bf16[256,512]{0,1:T(8,128)(2,1)S(1)}, u32[]{:S(2)}, u32[]{:S(2)}) collective-permute-start(bf16[256,512]{0,1:T(8,128)(2,1)S(1)} %collective-permute-done.21), channel_id=1, source_target_pairs={{0,32},{8,40},{16,48},{24,56},{32,0},{40,8},{48,16},{56,24},{64,96... | collective-permute-start | bytes 786440 | tf_op jit(solution)/shard_map/ppermute | solution.py:48
  669.5 6.6 fusion.85
  676.2 107.7 %collective-permute-start.23 = (bf16[256,512]{0,1:T(8,128)(2,1)S(1)}, bf16[256,512]{0,1:T(8,128)(2,1)S(1)}, u32[]{:S(2)}, u32[]{:S(2)}) collective-permute-start(bf16[256,512]{0,1:T(8,128)(2,1)S(1)} %collective-permute-done.22), channel_id=1, source_target_pairs={{0,64},{8,72},{16,80},{24,88},{32,96},{40,104},{48,112},{56,120},{... | collective-permute-start | bytes 786440 | tf_op jit(solution)/shard_map/ppermute | solution.py:48
  783.9 200.5 %while.24 = (s32[]{:T(128)}, f32[256,8,64]{0,2,1:T(8,128)S(1)}, f32[8,256]{1,0:T(8,128)S(1)}, s32[]{:T(128)}, s32[]{:T(128)}, /*index=5*/bf16[2,8192,8,64]{1,3,2...) while((s32[]{:T(128)}, f32[256,8,64]{0,2,1:T(8,128)S(1)}, ...), condition=%wide.region_9.10_spmd, body=%wide.region_6.9_spmd.sunk | while | flops 426934272 | bytes 44548372 | solution.py:176
  792.5 4.7 fusion.179
  805.8 4.7 fusion.179
  819.2 4.7 fusion.179
  832.6 4.7 fusion.179
  837.4 4.1 fusion.176
  846.0 4.7 fusion.179
  850.7 4.1 fusion.176
  859.3 4.7 fusion.179
  872.7 4.7 fusion.179
  886.1 4.7 fusion.179
  899.4 4.7 fusion.179
  904.2 4.1 fusion.176
  912.8 4.7 fusion.179
  926.2 4.7 fusion.179
  939.5 4.7 fusion.179
  952.9 4.7 fusion.179
  966.3 4.7 fusion.179
  971.1 4.1 fusion.176
  979.6 4.7 fusion.179
  984.7 13.7 %all_to_all.28 = bf16[2,256,512]{2,1,0:T(8,128)(2,1)S(1)} all-to-all(bf16[2,256,512]{2,1,0:T(8,128)(2,1)S(1)} %bitcast.251), channel_id=1, replica_groups=mesh['sp'=16,'fs'=4,'tp'=2] {'tp'}, dimensions={0} | all-to-all | bytes 1048576 | tf_op jit(solution)/shard_map/all_to_all | solution.py:194
  (324 shorter events, 239.5 us)
Async XLA Ops:
  6.5 400.7 %copy-start = (bf16[2,128,128]{2,1,0:T(8,128)(2,1)S(1)}, bf16[2,128,128]{2,1,0:T(8,128)(2,1)}, u32[]{:S(2)}) copy-start(bf16[2,128,128]{2,1,0:T(8,128)(2,1)} %param.28) | copy-start | bytes 196612
  6.5 3.0 copy-start.12
  6.5 78.6 %all-gather.8.cloned.1.call-start = ((), (), s32[]{:S(2)}) async-start(), calls=%async_computation.3 | async-start | bytes 9175040 | tf_op jit(solution)/shard_map/all_gather | solution.py:34
  9.5 7.2 copy-start.17
  11.1 8.2 all-to-all-start
  16.7 281.4 %all-gather.14.cloned.1.call-start = ((), (), s32[]{:S(2)}) async-start(), calls=%async_computation.6 | async-start | bytes 2621440 | tf_op jit(solution)/shard_map/all_gather | solution.py:190
  92.9 3.7 copy-start.21
  92.9 3.9 copy-start.11
  99.7 263.1 %copy-start.23 = (bf16[256]{0:T(256)(128)(2,1)S(1)}, bf16[256]{0:T(256)(128)(2,1)}, u32[]{:S(2)}) copy-start(bf16[256]{0:T(256)(128)(2,1)} %param.30) | copy-start | bytes 1540
  99.7 278.6 %copy-start.20 = (bf16[512]{0:T(512)(128)(2,1)S(1)}, bf16[512]{0:T(512)(128)(2,1)}, u32[]{:S(2)}) copy-start(bf16[512]{0:T(512)(128)(2,1)} %param.31) | copy-start | bytes 3076
  99.9 23.9 %collective-permute-start.1 = (bf16[2,512,8,64]{1,3,2,0:T(8,128)(2,1)S(1)}, bf16[2,512,8,64]{1,3,2,0:T(8,128)(2,1)S(1)}, u32[]{:S(2)}, u32[]{:S(2)}) collective-permute-start(bf16[2,512,8,64]{1,3,2,0:T(8,128)(2,1)S(1)} %pad_maximum_fusion.1), channel_id=1, source_target_pairs={{0,8},{8,16},{16,24},{24,32},{32,40},{40,48},{48,56},{56,64},{64,7... | collective-permute-start | bytes 3145736 | tf_op jit(solution)/shard_map/ppermute | solution.py:152
  123.8 1.0 copy-start.3
  124.8 24.2 %collective-permute-start.2 = (bf16[2,512,8,64]{1,3,2,0:T(8,128)(2,1)S(1)}, bf16[2,512,8,64]{1,3,2,0:T(8,128)(2,1)S(1)}, u32[]{:S(2)}, u32[]{:S(2)}) collective-permute-start(bf16[2,512,8,64]{1,3,2,0:T(8,128)(2,1)S(1)} %collective-permute-done.1), channel_id=1, source_target_pairs={{0,8},{8,16},{16,24},{24,32},{32,40},{40,48},{48,56},{56,64},{64,7... | collective-permute-start | bytes 3145736 | tf_op jit(solution)/shard_map/ppermute | solution.py:152
  149.0 1.0 copy-start.5
  149.9 25.5 %collective-permute-start.3 = (bf16[2,512,8,64]{1,3,2,0:T(8,128)(2,1)S(1)}, bf16[2,512,8,64]{1,3,2,0:T(8,128)(2,1)}, u32[]{:S(2)}, u32[]{:S(2)}) collective-permute-start(bf16[2,512,8,64]{1,3,2,0:T(8,128)(2,1)S(1)} %collective-permute-done.2), channel_id=1, source_target_pairs={{0,8},{8,16},{16,24},{24,32},{32,40},{40,48},{48,56},{56,64},{64,7... | collective-permute-start | bytes 3145736 | tf_op jit(solution)/shard_map/ppermute | solution.py:152
  175.4 25.1 %collective-permute-start.4 = (bf16[2,512,8,64]{1,3,2,0:T(8,128)(2,1)}, bf16[2,512,8,64]{1,3,2,0:T(8,128)(2,1)}, u32[]{:S(2)}, u32[]{:S(2)}) collective-permute-start(bf16[2,512,8,64]{1,3,2,0:T(8,128)(2,1)} %collective-permute-done.3), channel_id=1, source_target_pairs={{0,8},{8,16},{16,24},{24,32},{32,40},{40,48},{48,56},{56,64},{64,7... | collective-permute-start | bytes 3145736 | tf_op jit(solution)/shard_map/ppermute | solution.py:152
  181.1 204.1 %all-gather.10.cloned.1.call-start = ((), (), s32[]{:S(2)}) async-start(), calls=%async_computation.4 | async-start | bytes 1310720 | tf_op jit(solution)/shard_map/all_gather | solution.py:189
  200.5 24.1 %collective-permute-start.5 = (bf16[2,512,8,64]{1,3,2,0:T(8,128)(2,1)}, bf16[2,512,8,64]{1,3,2,0:T(8,128)(2,1)S(1)}, u32[]{:S(2)}, u32[]{:S(2)}) collective-permute-start(bf16[2,512,8,64]{1,3,2,0:T(8,128)(2,1)} %collective-permute-done.4), channel_id=1, source_target_pairs={{0,8},{8,16},{16,24},{24,32},{32,40},{40,48},{48,56},{56,64},{64,7... | collective-permute-start | bytes 3145736 | tf_op jit(solution)/shard_map/ppermute | solution.py:152
  224.6 1.0 copy-start.7
  225.6 22.8 %collective-permute-start.6 = (bf16[2,512,8,64]{1,3,2,0:T(8,128)(2,1)S(1)}, bf16[2,512,8,64]{1,3,2,0:T(8,128)(2,1)}, u32[]{:S(2)}, u32[]{:S(2)}) collective-permute-start(bf16[2,512,8,64]{1,3,2,0:T(8,128)(2,1)S(1)} %collective-permute-done.5), channel_id=1, source_target_pairs={{0,8},{8,16},{16,24},{24,32},{32,40},{40,48},{48,56},{56,64},{64,7... | collective-permute-start | bytes 3145736 | tf_op jit(solution)/shard_map/ppermute | solution.py:152
  248.4 22.5 %collective-permute-start.7 = (bf16[2,512,8,64]{1,3,2,0:T(8,128)(2,1)}, bf16[2,512,8,64]{1,3,2,0:T(8,128)(2,1)}, u32[]{:S(2)}, u32[]{:S(2)}) collective-permute-start(bf16[2,512,8,64]{1,3,2,0:T(8,128)(2,1)} %collective-permute-done.6), channel_id=1, source_target_pairs={{0,8},{8,16},{16,24},{24,32},{32,40},{40,48},{48,56},{56,64},{64,7... | collective-permute-start | bytes 3145736 | tf_op jit(solution)/shard_map/ppermute | solution.py:152
  254.0 745.3 %all-gather.16.cloned.1.call-start = ((), (), s32[]{:S(2)}) async-start(), calls=%async_computation.7 | async-start | bytes 6291456 | tf_op jit(solution)/shard_map/all_gather | solution.py:198
  270.9 21.6 %collective-permute-start.8 = (bf16[2,512,8,64]{1,3,2,0:T(8,128)(2,1)}, bf16[2,512,8,64]{1,3,2,0:T(8,128)(2,1)}, u32[]{:S(2)}, u32[]{:S(2)}) collective-permute-start(bf16[2,512,8,64]{1,3,2,0:T(8,128)(2,1)} %collective-permute-done.7), channel_id=1, source_target_pairs={{0,8},{8,16},{16,24},{24,32},{32,40},{40,48},{48,56},{56,64},{64,7... | collective-permute-start | bytes 3145736 | tf_op jit(solution)/shard_map/ppermute | solution.py:152
  292.5 21.6 %collective-permute-start.9 = (bf16[2,512,8,64]{1,3,2,0:T(8,128)(2,1)}, bf16[2,512,8,64]{1,3,2,0:T(8,128)(2,1)}, u32[]{:S(2)}, u32[]{:S(2)}) collective-permute-start(bf16[2,512,8,64]{1,3,2,0:T(8,128)(2,1)} %collective-permute-done.8), channel_id=1, source_target_pairs={{0,8},{8,16},{16,24},{24,32},{32,40},{40,48},{48,56},{56,64},{64,7... | collective-permute-start | bytes 3145736 | tf_op jit(solution)/shard_map/ppermute | solution.py:152
  298.0 704.9 %all-gather.12.cloned.1.call-start = ((), (), s32[]{:S(2)}) async-start(), calls=%async_computation.5 | async-start | bytes 3145728 | tf_op jit(solution)/shard_map/all_gather | solution.py:197
  314.1 21.6 %collective-permute-start.10 = (bf16[2,512,8,64]{1,3,2,0:T(8,128)(2,1)}, bf16[2,512,8,64]{1,3,2,0:T(8,128)(2,1)}, u32[]{:S(2)}, u32[]{:S(2)}) collective-permute-start(bf16[2,512,8,64]{1,3,2,0:T(8,128)(2,1)} %collective-permute-done.9), channel_id=1, source_target_pairs={{0,8},{8,16},{16,24},{24,32},{32,40},{40,48},{48,56},{56,64},{64,7... | collective-permute-start | bytes 3145736 | tf_op jit(solution)/shard_map/ppermute | solution.py:152
  335.7 21.6 %collective-permute-start.11 = (bf16[2,512,8,64]{1,3,2,0:T(8,128)(2,1)}, bf16[2,512,8,64]{1,3,2,0:T(8,128)(2,1)}, u32[]{:S(2)}, u32[]{:S(2)}) collective-permute-start(bf16[2,512,8,64]{1,3,2,0:T(8,128)(2,1)} %collective-permute-done.10), channel_id=1, source_target_pairs={{0,8},{8,16},{16,24},{24,32},{32,40},{40,48},{48,56},{56,64},{64,7... | collective-permute-start | bytes 3145736 | tf_op jit(solution)/shard_map/ppermute | solution.py:152
  357.3 25.0 %collective-permute-start.12 = (bf16[2,512,8,64]{1,3,2,0:T(8,128)(2,1)}, bf16[2,512,8,64]{1,3,2,0:T(8,128)(2,1)}, u32[]{:S(2)}, u32[]{:S(2)}) collective-permute-start(bf16[2,512,8,64]{1,3,2,0:T(8,128)(2,1)} %collective-permute-done.11), channel_id=1, source_target_pairs={{0,8},{8,16},{16,24},{24,32},{32,40},{40,48},{48,56},{56,64},{64,7... | collective-permute-start | bytes 3145736 | tf_op jit(solution)/shard_map/ppermute | solution.py:152
  382.3 18.6 %collective-permute-start.13 = (bf16[2,512,8,64]{1,3,2,0:T(8,128)(2,1)}, bf16[2,512,8,64]{1,3,2,0:T(8,128)(2,1)}, u32[]{:S(2)}, u32[]{:S(2)}) collective-permute-start(bf16[2,512,8,64]{1,3,2,0:T(8,128)(2,1)} %collective-permute-done.12), channel_id=1, source_target_pairs={{0,8},{8,16},{16,24},{24,32},{32,40},{40,48},{48,56},{56,64},{64,7... | collective-permute-start | bytes 3145736 | tf_op jit(solution)/shard_map/ppermute | solution.py:152
  387.9 19.3 %collective-permute-start = (bf16[16,256]{1,0:T(8,128)(2,1)S(1)}, bf16[16,256]{1,0:T(8,128)(2,1)S(1)}, u32[]{:S(2)}, u32[]{:S(2)}) collective-permute-start(bf16[16,256]{1,0:T(8,128)(2,1)S(1)} %slice.170), channel_id=1, source_target_pairs={{0,8},{8,16},{16,24},{24,32},{32,40},{40,48},{48,56},{56,64},{64,7... | collective-permute-start | bytes 24584 | tf_op jit(solution)/shard_map/ppermute | solution.py:44
  391.7 14.5 %copy-start.22 = (f32[64]{0:T(128)S(1)}, f32[64]{0:T(128)}, u32[]{:S(2)}) copy-start(f32[64]{0:T(128)} %param.25) | copy-start | bytes 772
  391.7 15.6 %copy-start.25 = (pred[256]{0:T(512)(128)(4,1)S(1)}, pred[256]{0:T(512)(128)(4,1)}, u32[]{:S(2)}) copy-start(pred[256]{0:T(512)(128)(4,1)} %get-tuple-element.149) | copy-start | bytes 772
  391.7 15.6 %copy-start.26 = (pred[256]{0:T(512)(128)(4,1)S(1)}, pred[256]{0:T(512)(128)(4,1)}, u32[]{:S(2)}) copy-start(pred[256]{0:T(512)(128)(4,1)} %get-tuple-element.140) | copy-start | bytes 772
  391.7 15.6 %copy-start.27 = (pred[256]{0:T(512)(128)(4,1)S(1)}, pred[256]{0:T(512)(128)(4,1)}, u32[]{:S(2)}) copy-start(pred[256]{0:T(512)(128)(4,1)} %get-tuple-element.141) | copy-start | bytes 772
  400.9 22.8 %collective-permute-start.14 = (bf16[2,512,8,64]{1,3,2,0:T(8,128)(2,1)}, bf16[2,512,8,64]{1,3,2,0:T(8,128)(2,1)S(1)}, u32[]{:S(2)}, u32[]{:S(2)}) collective-permute-start(bf16[2,512,8,64]{1,3,2,0:T(8,128)(2,1)} %collective-permute-done.13), channel_id=1, source_target_pairs={{0,8},{8,16},{16,24},{24,32},{32,40},{40,48},{48,56},{56,64},{64,7... | collective-permute-start | bytes 3145736 | tf_op jit(solution)/shard_map/ppermute | solution.py:152
  407.2 47.5 %collective-permute-start.16 = (bf16[256,8,64]{0,2,1:T(8,128)(2,1)}, bf16[256,8,64]{0,2,1:T(8,128)(2,1)}, u32[]{:S(2)}, u32[]{:S(2)}) collective-permute-start(bf16[256,8,64]{0,2,1:T(8,128)(2,1)} %get-tuple-element.132), channel_id=1, source_target_pairs={{0,8},{8,0},{16,24},{24,16},{32,40},{40,32},{48,56},{56,48},{64,72... | collective-permute-start | bytes 786440 | tf_op jit(solution)/shard_map/ppermute | solution.py:48
  407.3 21.5 %copy-start.19 = (f32[256]{0:T(256)S(1)}, f32[256]{0:T(256)}, u32[]{:S(2)}) copy-start(f32[256]{0:T(256)} %param.29) | copy-start | bytes 3076
  423.7 49.6 %copy-start.9 = (bf16[2,512,8,64]{1,3,2,0:T(8,128)(2,1)}, bf16[2,512,8,64]{1,3,2,0:T(8,128)(2,1)S(1)}, u32[]{:S(2)}) copy-start(bf16[2,512,8,64]{1,3,2,0:T(8,128)(2,1)S(1)} %collective-permute-done.14) | copy-start | bytes 3145732
  423.7 48.1 %collective-permute-start.15 = (bf16[2,512,8,64]{1,3,2,0:T(8,128)(2,1)S(1)}, bf16[2,512,8,64]{1,3,2,0:T(8,128)(2,1)}, u32[]{:S(2)}, u32[]{:S(2)}) collective-permute-start(bf16[2,512,8,64]{1,3,2,0:T(8,128)(2,1)S(1)} %collective-permute-done.14), channel_id=1, source_target_pairs={{0,8},{8,16},{16,24},{24,32},{32,40},{40,48},{48,56},{56,64},{64,7... | collective-permute-start | bytes 3145736 | tf_op jit(solution)/shard_map/ppermute | solution.py:152
  430.6 25.3 %all-to-all-start.1 = ((bf16[2,256,256]{2,1,0:T(8,128)(2,1)}), bf16[2,256,256]{2,1,0:T(8,128)(2,1)S(1)}, u32[]{:S(2)}, u32[]{:S(2)}) async-start(bf16[2,256,256]{2,1,0:T(8,128)(2,1)} %multiply_convert_fusion.3), calls=%async_computation.1 | async-start | bytes 524288 | tf_op jit(solution)/shard_map/all_to_all | solution.py:193
  454.6 9.6 collective-permute-start.17
  464.2 7.1 collective-permute-start.18
  471.3 40.9 %collective-permute-start.19 = (bf16[256,8,64]{0,2,1:T(8,128)(2,1)S(1)}, bf16[256,8,64]{0,2,1:T(8,128)(2,1)S(1)}, u32[]{:S(2)}, u32[]{:S(2)}) collective-permute-start(bf16[256,8,64]{0,2,1:T(8,128)(2,1)S(1)} %collective-permute-done.18), channel_id=1, source_target_pairs={{0,64},{8,72},{16,80},{24,88},{32,96},{40,104},{48,112},{56,120},{... | collective-permute-start | bytes 786440 | tf_op jit(solution)/shard_map/ppermute | solution.py:48
  478.7 5.6 copy-start.8
  482.9 4.4 copy-start.6
  484.3 3.1 copy-start.4
  487.3 1.8 copy-start.10
  503.3 17.5 %copy-start.2 = (bf16[2,16384,8,64]{1,3,2,0:T(8,128)(2,1)}, bf16[2,16384,8,64]{1,3,2,0:T(8,128)(2,1)S(1)}, u32[]{:S(2)}) copy-start(bf16[2,16384,8,64]{1,3,2,0:T(8,128)(2,1)S(1)} %constant_dynamic-update-slice_fusion) | copy-start | bytes 100663296
  512.3 8.6 copy-start.15
  512.3 8.6 copy-start.16
  512.3 8.6 copy-start.24
  561.6 13.5 %collective-permute-start.20 = (bf16[256,512]{0,1:T(8,128)(2,1)S(1)}, bf16[256,512]{0,1:T(8,128)(2,1)S(1)}, u32[]{:S(2)}, u32[]{:S(2)}) collective-permute-start(bf16[256,512]{0,1:T(8,128)(2,1)S(1)} %bitcast.256), channel_id=1, source_target_pairs={{0,8},{8,0},{16,24},{24,16},{32,40},{40,32},{48,56},{56,48},{64,72... | collective-permute-start | bytes 786440 | tf_op jit(solution)/shard_map/ppermute | solution.py:48
  575.0 39.4 %collective-permute-start.21 = (bf16[256,512]{0,1:T(8,128)(2,1)S(1)}, bf16[256,512]{0,1:T(8,128)(2,1)S(1)}, u32[]{:S(2)}, u32[]{:S(2)}) collective-permute-start(bf16[256,512]{0,1:T(8,128)(2,1)S(1)} %collective-permute-done.20), channel_id=1, source_target_pairs={{0,16},{8,24},{16,0},{24,8},{32,48},{40,56},{48,32},{56,40},{64,80... | collective-permute-start | bytes 786440 | tf_op jit(solution)/shard_map/ppermute | solution.py:48
  614.5 61.7 %collective-permute-start.22 = (bf16[256,512]{0,1:T(8,128)(2,1)S(1)}, bf16[256,512]{0,1:T(8,128)(2,1)S(1)}, u32[]{:S(2)}, u32[]{:S(2)}) collective-permute-start(bf16[256,512]{0,1:T(8,128)(2,1)S(1)} %collective-permute-done.21), channel_id=1, source_target_pairs={{0,32},{8,40},{16,48},{24,56},{32,0},{40,8},{48,16},{56,24},{64,96... | collective-permute-start | bytes 786440 | tf_op jit(solution)/shard_map/ppermute | solution.py:48
  669.5 114.4 %copy-start.14 = (bf16[256,8,64]{0,2,1:T(8,128)(2,1)S(1)}, bf16[256,8,64]{0,2,1:T(8,128)(2,1)}, u32[]{:S(2)}) copy-start(bf16[256,8,64]{0,2,1:T(8,128)(2,1)} %get-tuple-element.311) | copy-start | bytes 786436
  676.2 308.3 %collective-permute-start.23 = (bf16[256,512]{0,1:T(8,128)(2,1)S(1)}, bf16[256,512]{0,1:T(8,128)(2,1)S(1)}, u32[]{:S(2)}, u32[]{:S(2)}) collective-permute-start(bf16[256,512]{0,1:T(8,128)(2,1)S(1)} %collective-permute-done.22), channel_id=1, source_target_pairs={{0,64},{8,72},{16,80},{24,88},{32,96},{40,104},{48,112},{56,120},{... | collective-permute-start | bytes 786440 | tf_op jit(solution)/shard_map/ppermute | solution.py:48
  984.4 14.7 %copy-start.18 = (f32[2,1,512]{2,1,0:T(1,128)S(1)}, f32[2,1,512]{2,1,0:T(1,128)}, u32[]{:S(2)}) copy-start(f32[2,1,512]{2,1,0:T(1,128)} %convert_element_type.154) | copy-start | bytes 12292
  999.1 3.8 copy-start.13
  999.4 6.8 copy-start.1
Sparse Core Ops, SparseCore 0:
  9.6 75.4 all-gather.7
  181.2 33.9 all-gather.13
  254.1 27.9 all-gather.9
  298.2 25.5 all-gather.15
  385.4 29.1 all-gather.11
